TPU v7x, 32 devices: a whole 2x2x4 slice. The times are simulated.
32 devices in a mesh: grp: 2 (over x), sp: 4 (over z), tp: 4 (over y, core).
Axes of the slice: x: 2, y: 2, z: 4, core: 2. Of those that a mesh axis runs over, the one named last changes fastest.
Arguments:
- tokens: bfloat16 [1792, 4096], P(('grp', 'sp'), 'tp'), parts along dimension 0, may hold values from -130 to 130
- rms_gain: float32 [2, 4096], replicated, may hold values from 0.1 to 1.9
- w_value: bfloat16 [2, 4096, 2048], P(None, 'sp', 'tp'), may hold values from -0.09375 to 0.09375
- w_gate: bfloat16 [2, 4096, 2048], P(None, 'sp', 'tp'), may hold values from -0.09375 to 0.09375
- taps: float32 [2, 31, 2048], P(None, None, 'tp'), may hold values from -8 to 8
- ln_gain: float32 [2, 2048], P(None, 'tp'), may hold values from 0.1 to 1.9
- ln_bias: float32 [2, 2048], P(None, 'tp'), may hold values from -3 to 3
- w_out: bfloat16 [2, 2048, 4096], P(None, 'sp', 'tp'), may hold values from -0.125 to 0.125
Outputs:
- result: bfloat16 [1792, 4096], P(('grp', 'sp'), 'tp'), parts along dimension 0
There are 2 independent parts, one for each index of `grp`. A program takes and returns all parts, laid end to end along the dimension named above; an argument that names none is the same for every part. Nothing has to cross between parts.
All inputs are finite; a program needn't handle non-finite values.
Results may differ from a plain program's by a relative error of at most 0.009.
Values may be sent and summed in bfloat16 or wider, within the bound.
A program may use at most 64 MiB of HBM per device.

v0:
```python
import jax
import jax.numpy as jnp
from jax import lax
from jax.sharding import PartitionSpec as P

CH = 2048


def passed_along(block, axis, distance):
    devices = range(lax.axis_size(axis))
    route = [(i - distance, i) for i in devices if i - distance in devices]
    return lax.ppermute(block, axis, route)


def project_in(weight, columns):
    return lax.dot_general(
        weight, columns, (((0,), (1,)), ((), ())), preferred_element_type=jnp.float32
    )


def project_out(rows, weight):
    return lax.dot_general(
        rows, weight, (((0,), (0,)), ((), ())), preferred_element_type=jnp.float32
    )


def norm_rows(wide, gain):
    return (wide * lax.rsqrt(jnp.mean(wide * wide, axis=1, keepdims=True) + 1e-06) * gain).astype(
        jnp.bfloat16
    )


def shards(tokens, rms_gain, w_value, w_gate, taps, ln_gain, ln_bias, w_out):
    layers = w_value.shape[0]
    tok_rows = tokens.shape[0]
    chans = w_value.shape[2]
    reach = taps.shape[1]
    current = tokens
    for layer in range(layers):
        gain = rms_gain[layer]
        whole_rows = lax.all_gather(current, "tp", axis=1, tiled=True)
        normed = norm_rows(whole_rows.astype(jnp.float32), gain)
        value_t = project_in(lax.all_gather(w_value[layer], "sp", axis=0, tiled=True), normed)
        gate_t = project_in(lax.all_gather(w_gate[layer], "sp", axis=0, tiled=True), normed)
        glu_t = (value_t * jax.nn.sigmoid(gate_t)).astype(jnp.bfloat16)
        earlier = passed_along(glu_t[:, tok_rows - (reach - 1) :], "sp", 1)
        extended = jnp.concatenate([earlier, glu_t], axis=1).astype(jnp.float32)
        layer_taps = taps[layer]
        conv = jnp.zeros((chans, tok_rows), jnp.float32)
        for k in range(reach):
            conv = conv + layer_taps[k][:, None] * extended[:, k : k + tok_rows]
        total, total_sq = lax.psum((jnp.sum(conv, axis=0), jnp.sum(conv * conv, axis=0)), "tp")
        mean = total / CH
        var = total_sq / CH - mean * mean
        shaped = (conv - mean[None, :]) * lax.rsqrt(var + 1e-05)[None, :] * ln_gain[layer][
            :, None
        ] + ln_bias[layer][:, None]
        act_t = jax.nn.silu(shaped).astype(jnp.bfloat16)
        act_all = lax.all_gather(act_t, "tp", axis=0, tiled=True)
        branch = project_out(act_all, lax.all_gather(w_out[layer], "sp", axis=0, tiled=True))
        current = (current.astype(jnp.float32) + branch).astype(jnp.bfloat16)
    return current


def solution(mesh):
    return jax.shard_map(
        shards,
        mesh=mesh,
        in_specs=(
            P(("grp", "sp"), "tp"),
            P(),
            P(None, "sp", "tp"),
            P(None, "sp", "tp"),
            P(None, None, "tp"),
            P(None, "tp"),
            P(None, "tp"),
            P(None, "sp", "tp"),
        ),
        out_specs=P(("grp", "sp"), "tp"),
        check_vma=False,
    )
```

profile of v0, /device:TPU:0, one launch (start us, length us, event | category | flops | bytes accessed | tf_op | source)
XLA Modules:
  0.0 555.3 jit_solution(11916564640636365866)
XLA Ops:
  7.3 3.0 fusion.142
  11.9 3.0 fusion.140
  15.2 17.5 %all-gather.15.cloned.1.call-done = bf16[224,4096]{1,0:T(8,128)(2,1)} async-done(((bf16[224,1024]{1,0:T(8,128)(2,1)}), bf16[224,4096]{1,0:T(8,128)(2,1)}) %all-gather.15.cloned.1.call-update) | async-done | bytes 1835024 | tf_op jit(solution)/shard_map/all_gather | solution.py:41
  32.8 1.9 fusion.12
  34.7 80.4 %all-gather.21.cloned.1.call-done = bf16[1,4096,512]{2,1,0:T(8,128)(2,1)} async-done(((bf16[1,1024,512]{2,1,0:T(8,128)(2,1)}), bf16[1,4096,512]{2,1,0:T(8,128)(2,1)}) %all-gather.21.cloned.1.call-update) | async-done | bytes 4194320 | tf_op jit(solution)/shard_map/all_gather | solution.py:44
  115.1 4.1 fusion.57
  119.2 76.7 %all-gather.19.cloned.1.call-done = bf16[1,4096,512]{2,1,0:T(8,128)(2,1)} async-done(((bf16[1,1024,512]{2,1,0:T(8,128)(2,1)}), bf16[1,4096,512]{2,1,0:T(8,128)(2,1)}) %all-gather.19.cloned.1.call-update) | async-done | bytes 4194320 | tf_op jit(solution)/shard_map/all_gather | solution.py:43
  195.9 3.3 fusion.66
  202.2 2.4 fusion.137
  204.6 6.3 %all-reduce.1 = (f32[224]{0:T(256)S(1)}, f32[224]{0:T(256)S(1)}) all-reduce(f32[224]{0:T(256)S(1)} %get-tuple-element.8, f32[224]{0:T(256)S(1)} %get-tuple-element.7), channel_id=1, replica_groups=mesh['grp'=2,'sp'=4,'tp'=4] {'tp'}, use_global_device_ids=true, to_apply=%region_4.0 | all-reduce | flops 448 | bytes 3584 | tf_op jit(solution)/shard_map/psum | solution.py:52
  211.2 9.1 %all_gather.33 = bf16[2048,224]{0,1:T(8,128)(2,1)S(1)} all-gather(bf16[512,224]{0,1:T(8,128)(2,1)S(1)} %multiply_convert_fusion.1), channel_id=1, replica_groups=mesh['grp'=2,'sp'=4,'tp'=4] {'tp'}, dimensions={0}, use_global_device_ids=true | all-gather | bytes 1146880 | tf_op jit(solution)/shard_map/all_gather | solution.py:59
  220.3 56.3 %all-gather.23.cloned.1.call-done = bf16[1,2048,1024]{2,1,0:T(8,128)(2,1)} async-done(((bf16[1,512,1024]{2,1,0:T(8,128)(2,1)}), bf16[1,2048,1024]{2,1,0:T(8,128)(2,1)}) %all-gather.23.cloned.1.call-update) | async-done | bytes 4194320 | tf_op jit(solution)/shard_map/all_gather | solution.py:60
  276.6 4.1 fusion.27
  282.8 17.7 %all-gather.17.cloned.1.call-done = bf16[224,4096]{1,0:T(8,128)(2,1)} async-done(((bf16[224,1024]{1,0:T(8,128)(2,1)}), bf16[224,4096]{1,0:T(8,128)(2,1)}) %all-gather.17.cloned.1.call-update) | async-done | bytes 1835024 | tf_op jit(solution)/shard_map/all_gather | solution.py:41
  300.5 1.9 fusion.15
  302.4 80.2 %all-gather.27.cloned.1.call-done = bf16[1,4096,512]{2,1,0:T(8,128)(2,1)} async-done(((bf16[1,1024,512]{2,1,0:T(8,128)(2,1)}), bf16[1,4096,512]{2,1,0:T(8,128)(2,1)}) %all-gather.27.cloned.1.call-update) | async-done | bytes 4194320 | tf_op jit(solution)/shard_map/all_gather | solution.py:44
  382.7 4.1 fusion.51
  386.8 76.7 %all-gather.25.cloned.1.call-done = bf16[1,4096,512]{2,1,0:T(8,128)(2,1)} async-done(((bf16[1,1024,512]{2,1,0:T(8,128)(2,1)}), bf16[1,4096,512]{2,1,0:T(8,128)(2,1)}) %all-gather.25.cloned.1.call-update) | async-done | bytes 4194320 | tf_op jit(solution)/shard_map/all_gather | solution.py:43
  463.5 3.3 fusion.69
  469.8 2.4 fusion.136
  472.2 6.3 %all-reduce = (f32[224]{0:T(256)S(1)}, f32[224]{0:T(256)S(1)}) all-reduce(f32[224]{0:T(256)S(1)} %get-tuple-element.6, f32[224]{0:T(256)S(1)} %get-tuple-element.5), channel_id=1, replica_groups=mesh['grp'=2,'sp'=4,'tp'=4] {'tp'}, use_global_device_ids=true, to_apply=%region_9.10 | all-reduce | flops 448 | bytes 3584 | tf_op jit(solution)/shard_map/psum | solution.py:52
  478.8 9.1 %all_gather.38 = bf16[2048,224]{0,1:T(8,128)(2,1)S(1)} all-gather(bf16[512,224]{0,1:T(8,128)(2,1)S(1)} %multiply_convert_fusion), channel_id=1, replica_groups=mesh['grp'=2,'sp'=4,'tp'=4] {'tp'}, dimensions={0}, use_global_device_ids=true | all-gather | bytes 1146880 | tf_op jit(solution)/shard_map/all_gather | solution.py:59
  487.9 56.5 %all-gather.29.cloned.1.call-done = bf16[1,2048,1024]{2,1,0:T(8,128)(2,1)} async-done(((bf16[1,512,1024]{2,1,0:T(8,128)(2,1)}), bf16[1,2048,1024]{2,1,0:T(8,128)(2,1)}) %all-gather.29.cloned.1.call-update) | async-done | bytes 4194320 | tf_op jit(solution)/shard_map/all_gather | solution.py:60
  544.3 4.1 fusion.24
  (56 shorter events, 11.0 us)
Async XLA Ops:
  6.5 3.9 copy-start
  6.5 26.2 %all-gather.15.cloned.1.call-start = ((), (), s32[]{:S(2)}) async-start(), calls=%async_computation | async-start | bytes 2293760 | tf_op jit(solution)/shard_map/all_gather | solution.py:41
  7.3 107.8 %all-gather.21.cloned.1.call-start = ((), (), s32[]{:S(2)}) async-start(), calls=%async_computation.3 | async-start | bytes 5242880 | tf_op jit(solution)/shard_map/all_gather | solution.py:44
  10.3 185.6 %all-gather.19.cloned.1.call-start = ((), (), s32[]{:S(2)}) async-start(), calls=%async_computation.2 | async-start | bytes 5242880 | tf_op jit(solution)/shard_map/all_gather | solution.py:43
  11.9 3.2 copy-start.7
  11.9 3.2 copy-start.5
  11.9 3.3 copy-start.6
  11.9 264.7 %all-gather.23.cloned.1.call-start = ((), (), s32[]{:S(2)}) async-start(), calls=%async_computation.4 | async-start | bytes 5242880 | tf_op jit(solution)/shard_map/all_gather | solution.py:60
  15.0 285.5 %all-gather.17.cloned.1.call-start = ((), (), s32[]{:S(2)}) async-start(), calls=%async_computation.1 | async-start | bytes 2293760 | tf_op jit(solution)/shard_map/all_gather | solution.py:41
  115.1 80.8 %copy-start.1 = (bf16[224,4096]{1,0:T(8,128)(2,1)S(1)}, bf16[224,4096]{1,0:T(8,128)(2,1)}, u32[]{:S(2)}) copy-start(bf16[224,4096]{1,0:T(8,128)(2,1)} %all-gather.15.cloned.1.call-done) | copy-start | bytes 5505028
  119.2 81.4 %copy-start.8 = (f32[2,512]{1,0:T(2,128)S(1)}, f32[2,512]{1,0:T(2,128)}, u32[]{:S(2)}) copy-start(f32[2,512]{1,0:T(2,128)} %param.14) | copy-start | bytes 12292
  199.3 2.9 collective-permute-start
  202.2 74.4 %copy-start.3 = (bf16[224,1024]{1,0:T(8,128)(2,1)S(1)}, bf16[224,1024]{1,0:T(8,128)(2,1)}, u32[]{:S(2)}) copy-start(bf16[224,1024]{1,0:T(8,128)(2,1)} %param.8) | copy-start | bytes 1376260
  280.7 101.9 %all-gather.27.cloned.1.call-start = ((), (), s32[]{:S(2)}) async-start(), calls=%async_computation.6 | async-start | bytes 5242880 | tf_op jit(solution)/shard_map/all_gather | solution.py:44
  281.3 182.2 %all-gather.25.cloned.1.call-start = ((), (), s32[]{:S(2)}) async-start(), calls=%async_computation.5 | async-start | bytes 5242880 | tf_op jit(solution)/shard_map/all_gather | solution.py:43
  282.1 262.3 %all-gather.29.cloned.1.call-start = ((), (), s32[]{:S(2)}) async-start(), calls=%async_computation.7 | async-start | bytes 5242880 | tf_op jit(solution)/shard_map/all_gather | solution.py:60
  382.7 80.8 %copy-start.2 = (bf16[224,4096]{1,0:T(8,128)(2,1)S(1)}, bf16[224,4096]{1,0:T(8,128)(2,1)}, u32[]{:S(2)}) copy-start(bf16[224,4096]{1,0:T(8,128)(2,1)} %all-gather.17.cloned.1.call-done) | copy-start | bytes 5505028
  466.9 2.9 collective-permute-start.1
  469.8 74.5 %copy-start.4 = (bf16[224,1024]{1,0:T(8,128)(2,1)S(1)}, bf16[224,1024]{1,0:T(8,128)(2,1)}, u32[]{:S(2)}) copy-start(bf16[224,1024]{1,0:T(8,128)(2,1)} %fusion.27) | copy-start | bytes 1376260
Sparse Core Ops, SparseCore 0:
  8.9 23.8 all-gather.14
  34.3 80.7 all-gather.20
  116.7 79.2 all-gather.18
  197.3 79.2 all-gather.22
  280.8 19.5 all-gather.16
  301.9 80.7 all-gather.26
  384.2 79.2 all-gather.24
  465.1 79.2 all-gather.28
where the time goes:
time: 556 us; the launch traced here: 555 us
  waiting for transfers between devices  468 us (84%)
  blocking collectives  30.7 us (6%)
  matrix products  23.1 us (4%)
  between operations  13.7 us (2%)
  other arithmetic  9.31 us (2%)
  local copies, waits for them, and re-layouts  7.75 us (1%)
    all_gather x2, waiting for transfers between devices, shards(): lax.all_gather(w_gate[layer], 'sp', axis=0, tiled=True)  161 us
    all_gather x2, waiting for transfers between devices, shards(): lax.all_gather(w_value[layer], 'sp', axis=0, tiled=True)  153 us
    all_gather x2, waiting for transfers between devices, shards(): lax.all_gather(w_out[layer], 'sp', axis=0, tiled=True)  113 us
    all_gather x2, waiting for transfers between devices, shards(): whole_rows = lax.all_gather(current, 'tp', axis=1, tiled=True)  35.2 us
    all_gather x2, blocking collectives, shards(): act_all = lax.all_gather(act_t, 'tp', axis=0, tiled=True)  18.2 us
    dot_general x4, matrix products, project_in(): lax.dot_general(weight, columns, (((0,), (1,)), ((), ())), preferred_elem...  14.9 us
    psum x2, blocking collectives, shards(): lax.psum((jnp.sum(conv, axis=0), jnp.sum(conv * conv, axis=0)), 'tp')  12.5 us
  transfers between devices with their start and end apart: 10, of which 10 were waited for; matrix products, arithmetic and copies ran while one was open for 6% of the time, Pallas kernels for 0%

commit v1 on v0

--- a/solution.py
+++ b/solution.py
@@ -38,7 +38,14 @@
     current = tokens
     for layer in range(layers):
         gain = rms_gain[layer]
-        whole_rows = lax.all_gather(current, "tp", axis=1, tiled=True)
+        ring = [current]
+        for hop in range(3):
+            ring.append(lax.ppermute(ring[-1], "tp", [(dev, (dev + 1) % 4) for dev in range(4)]))
+        whole_rows = jnp.roll(
+            jnp.concatenate(ring[::-1], axis=1),
+            (lax.axis_index("tp") + 1) * ring[0].shape[1],
+            axis=1,
+        )
         normed = norm_rows(whole_rows.astype(jnp.float32), gain)
         value_t = project_in(lax.all_gather(w_value[layer], "sp", axis=0, tiled=True), normed)
         gate_t = project_in(lax.all_gather(w_gate[layer], "sp", axis=0, tiled=True), normed)

time: 556 us -> 508 us (0.914)
  waiting for transfers between devices: 468 us -> 412 us
  other arithmetic: 9.31 us -> 17.9 us
    all_gather x2, waiting for transfers between devices: 161 us -> 94.1 us  [shards(): lax.all_gather(w_gate[layer], 'sp', axis=0, tiled=True)]
    ppermute x0 -> x6, waiting for transfers between devices: none -> 47.5 us  [shards(): lax.ppermute(ring[-1], 'tp', [(dev, (dev + 1) % 4) for dev in range(4)])]
    all_gather x2 -> x0, waiting for transfers between devices: 35.2 us -> none  [shards(): whole_rows = lax.all_gather(current, 'tp', axis=1, tiled=True)]
    reduce_sum x2, other arithmetic: 3.88 us -> 12.5 us  [norm_rows(): jnp.mean(wide * wide, axis=1, keepdims=True) + 1e-06]
  transfers between devices with their start and end apart: 10 -> 14, of which waited for: 10 -> 14; matrix products, arithmetic and copies ran while one was open for 6% -> 8% of each run, Pallas kernels for 0% -> 0%
where the time goes in v1:
time: 508 us
  waiting for transfers between devices  412 us (81%)
  blocking collectives  30.7 us (6%)
  matrix products  21.7 us (4%)
  other arithmetic  17.9 us (4%)
  between operations  13.8 us (3%)
  local copies, waits for them, and re-layouts  8.1 us (2%)
    all_gather x2, waiting for transfers between devices, shards(): lax.all_gather(w_value[layer], 'sp', axis=0, tiled=True)  154 us
    all_gather x2, waiting for transfers between devices, shards(): lax.all_gather(w_out[layer], 'sp', axis=0, tiled=True)  113 us
    all_gather x2, waiting for transfers between devices, shards(): lax.all_gather(w_gate[layer], 'sp', axis=0, tiled=True)  94.1 us
    ppermute x6, waiting for transfers between devices, shards(): lax.ppermute(ring[-1], 'tp', [(dev, (dev + 1) % 4) for dev in range(4)])  47.5 us
    all_gather x2, blocking collectives, shards(): act_all = lax.all_gather(act_t, 'tp', axis=0, tiled=True)  18.2 us
    dot_general x4, matrix products, project_in(): lax.dot_general(weight, columns, (((0,), (1,)), ((), ())), preferred_elem...  14.4 us
    psum x2, blocking collectives, shards(): lax.psum((jnp.sum(conv, axis=0), jnp.sum(conv * conv, axis=0)), 'tp')  12.5 us
    reduce_sum x2, other arithmetic, norm_rows(): jnp.mean(wide * wide, axis=1, keepdims=True) + 1e-06  12.5 us
  transfers between devices with their start and end apart: 14, of which 14 were waited for; matrix products, arithmetic and copies ran while one was open for 8% of the time, Pallas kernels for 0%

profile of v1, /device:TPU:0, one launch (start us, length us, event | category | flops | bytes accessed | tf_op | source)
XLA Modules:
  0.0 508.0 jit_solution(1724059352905296232)
XLA Ops:
  16.4 8.1 %collective-permute-done = bf16[224,1024]{1,0:T(8,128)(2,1)S(1)} collective-permute-done((bf16[224,1024]{1,0:T(8,128)(2,1)S(1)}, bf16[224,1024]{1,0:T(8,128)(2,1)S(1)}, u32[]{:S(2)}, u32[]{:S(2)}) %collective-permute-start) | collective-permute-done | bytes 458784 | tf_op jit(solution)/shard_map/ppermute | solution.py:43
  24.6 7.8 %collective-permute-done.1 = bf16[224,1024]{1,0:T(8,128)(2,1)S(1)} collective-permute-done((bf16[224,1024]{1,0:T(8,128)(2,1)S(1)}, bf16[224,1024]{1,0:T(8,128)(2,1)S(1)}, u32[]{:S(2)}, u32[]{:S(2)}) %collective-permute-start.1) | collective-permute-done | bytes 458784 | tf_op jit(solution)/shard_map/ppermute | solution.py:43
  32.5 7.9 %collective-permute-done.2 = bf16[224,1024]{1,0:T(8,128)(2,1)} collective-permute-done((bf16[224,1024]{1,0:T(8,128)(2,1)S(1)}, bf16[224,1024]{1,0:T(8,128)(2,1)}, u32[]{:S(2)}, u32[]{:S(2)}) %collective-permute-start.2) | collective-permute-done | bytes 458784 | tf_op jit(solution)/shard_map/ppermute | solution.py:43
  40.4 6.4 %fusion.12 = (f32[224]{0:T(256)S(1)}, bf16[224,4096]{1,0:T(8,128)(2,1)S(1)}) fusion(s32[]{:T(128)S(6)} %select_n.13, bf16[224,1024]{1,0:T(8,128)(2,1)S(1)} %copy-done.1, bf16[224,1024]{1,0:T(8,128)(2,1)S(1)} %collective-permute-done, bf16[224,1024]{1,0:T(8,128)(2,1)S(1)} %collective-permute-done.1, bf16[224,1024]{1,0:T(8,128)(2,1)} %collective-permute-done.2), kind=kLoop, calls=%fused_computation.16 | loop fusion | flops 17432352 | bytes 3670916 | tf_op jit(solution)/shard_map/reduce_sum | solution.py:28
  46.9 46.5 %all-gather.15.cloned.1.call-done = bf16[1,4096,512]{2,1,0:T(8,128)(2,1)} async-done(((bf16[1,1024,512]{2,1,0:T(8,128)(2,1)}), bf16[1,4096,512]{2,1,0:T(8,128)(2,1)}) %all-gather.15.cloned.1.call-update) | async-done | bytes 4194320 | tf_op jit(solution)/shard_map/all_gather | solution.py:51
  93.4 3.4 fusion.71
  96.9 77.4 %all-gather.13.cloned.1.call-done = bf16[1,4096,512]{2,1,0:T(8,128)(2,1)} async-done(((bf16[1,1024,512]{2,1,0:T(8,128)(2,1)}), bf16[1,4096,512]{2,1,0:T(8,128)(2,1)}) %all-gather.13.cloned.1.call-update) | async-done | bytes 4194320 | tf_op jit(solution)/shard_map/all_gather | solution.py:50
  174.2 3.3 fusion.80
  183.0 6.3 %all-reduce.1 = (f32[224]{0:T(256)S(1)}, f32[224]{0:T(256)S(1)}) all-reduce(f32[224]{0:T(256)S(1)} %get-tuple-element.9, f32[224]{0:T(256)S(1)} %get-tuple-element.8), channel_id=1, replica_groups=mesh['grp'=2,'sp'=4,'tp'=4] {'tp'}, use_global_device_ids=true, to_apply=%region_4.6 | all-reduce | flops 448 | bytes 3584 | tf_op jit(solution)/shard_map/psum | solution.py:59
  189.5 9.1 %all_gather.26 = bf16[2048,224]{0,1:T(8,128)(2,1)S(1)} all-gather(bf16[512,224]{0,1:T(8,128)(2,1)S(1)} %multiply_convert_fusion.1), channel_id=1, replica_groups=mesh['grp'=2,'sp'=4,'tp'=4] {'tp'}, dimensions={0}, use_global_device_ids=true | all-gather | bytes 1146880 | tf_op jit(solution)/shard_map/all_gather | solution.py:66
  198.6 56.5 %all-gather.17.cloned.1.call-done = bf16[1,2048,1024]{2,1,0:T(8,128)(2,1)} async-done(((bf16[1,512,1024]{2,1,0:T(8,128)(2,1)}), bf16[1,2048,1024]{2,1,0:T(8,128)(2,1)}) %all-gather.17.cloned.1.call-update) | async-done | bytes 4194320 | tf_op jit(solution)/shard_map/all_gather | solution.py:67
  255.1 3.3 fusion.41
  258.5 7.9 %collective-permute-done.4 = bf16[224,1024]{1,0:T(8,128)(2,1)S(1)} collective-permute-done((bf16[224,1024]{1,0:T(8,128)(2,1)S(1)}, bf16[224,1024]{1,0:T(8,128)(2,1)S(1)}, u32[]{:S(2)}, u32[]{:S(2)}) %collective-permute-start.4) | collective-permute-done | bytes 458784 | tf_op jit(solution)/shard_map/ppermute | solution.py:43
  266.3 7.9 %collective-permute-done.5 = bf16[224,1024]{1,0:T(8,128)(2,1)S(1)} collective-permute-done((bf16[224,1024]{1,0:T(8,128)(2,1)S(1)}, bf16[224,1024]{1,0:T(8,128)(2,1)S(1)}, u32[]{:S(2)}, u32[]{:S(2)}) %collective-permute-start.5) | collective-permute-done | bytes 458784 | tf_op jit(solution)/shard_map/ppermute | solution.py:43
  274.3 7.9 %collective-permute-done.6 = bf16[224,1024]{1,0:T(8,128)(2,1)S(1)} collective-permute-done((bf16[224,1024]{1,0:T(8,128)(2,1)S(1)}, bf16[224,1024]{1,0:T(8,128)(2,1)S(1)}, u32[]{:S(2)}, u32[]{:S(2)}) %collective-permute-start.6) | collective-permute-done | bytes 458784 | tf_op jit(solution)/shard_map/ppermute | solution.py:43
  282.2 6.0 %fusion.15 = (f32[224]{0:T(256)S(1)}, bf16[224,4096]{1,0:T(8,128)(2,1)S(1)}) fusion(s32[]{:T(128)S(6)} %select_n.13, bf16[224,1024]{1,0:T(8,128)(2,1)S(1)} %fusion.41, bf16[224,1024]{1,0:T(8,128)(2,1)S(1)} %collective-permute-done.4, bf16[224,1024]{1,0:T(8,128)(2,1)S(1)} %collective-permute-done.5, bf16[224,1024]{1,0:T(8,128)(2,1)S(1)} %collective-permute-done.6), kind=kLoop, calls=%fused_computation.19 | loop fusion | flops 17432352 | bytes 3670916 | tf_op jit(solution)/shard_map/reduce_sum | solution.py:28
  288.2 47.6 %all-gather.21.cloned.1.call-done = bf16[1,4096,512]{2,1,0:T(8,128)(2,1)} async-done(((bf16[1,1024,512]{2,1,0:T(8,128)(2,1)}), bf16[1,4096,512]{2,1,0:T(8,128)(2,1)}) %all-gather.21.cloned.1.call-update) | async-done | bytes 4194320 | tf_op jit(solution)/shard_map/all_gather | solution.py:51
  335.8 4.2 fusion.65
  339.9 76.5 %all-gather.19.cloned.1.call-done = bf16[1,4096,512]{2,1,0:T(8,128)(2,1)} async-done(((bf16[1,1024,512]{2,1,0:T(8,128)(2,1)}), bf16[1,4096,512]{2,1,0:T(8,128)(2,1)}) %all-gather.19.cloned.1.call-update) | async-done | bytes 4194320 | tf_op jit(solution)/shard_map/all_gather | solution.py:50
  416.4 3.4 fusion.83
  425.2 6.3 %all-reduce = (f32[224]{0:T(256)S(1)}, f32[224]{0:T(256)S(1)}) all-reduce(f32[224]{0:T(256)S(1)} %get-tuple-element.7, f32[224]{0:T(256)S(1)} %get-tuple-element.6), channel_id=1, replica_groups=mesh['grp'=2,'sp'=4,'tp'=4] {'tp'}, use_global_device_ids=true, to_apply=%region_9.11 | all-reduce | flops 448 | bytes 3584 | tf_op jit(solution)/shard_map/psum | solution.py:59
  431.8 9.1 %all_gather.30 = bf16[2048,224]{0,1:T(8,128)(2,1)S(1)} all-gather(bf16[512,224]{0,1:T(8,128)(2,1)S(1)} %multiply_convert_fusion), channel_id=1, replica_groups=mesh['grp'=2,'sp'=4,'tp'=4] {'tp'}, dimensions={0}, use_global_device_ids=true | all-gather | bytes 1146880 | tf_op jit(solution)/shard_map/all_gather | solution.py:66
  440.9 56.3 %all-gather.23.cloned.1.call-done = bf16[1,2048,1024]{2,1,0:T(8,128)(2,1)} async-done(((bf16[1,512,1024]{2,1,0:T(8,128)(2,1)}), bf16[1,2048,1024]{2,1,0:T(8,128)(2,1)}) %all-gather.23.cloned.1.call-update) | async-done | bytes 4194320 | tf_op jit(solution)/shard_map/all_gather | solution.py:67
  497.1 4.1 fusion.38
  (56 shorter events, 21.1 us)
Async XLA Ops:
  6.5 3.3 copy-start
  6.5 86.9 %all-gather.15.cloned.1.call-start = ((), (), s32[]{:S(2)}) async-start(), calls=%async_computation.1 | async-start | bytes 5242880 | tf_op jit(solution)/shard_map/all_gather | solution.py:51
  9.8 164.4 %all-gather.13.cloned.1.call-start = ((), (), s32[]{:S(2)}) async-start(), calls=%async_computation | async-start | bytes 5242880 | tf_op jit(solution)/shard_map/all_gather | solution.py:50
  11.4 4.4 copy-start.1
  11.4 13.1 %copy-start.3 = (f32[2,4096]{1,0:T(2,128)S(1)}, f32[2,4096]{1,0:T(2,128)}, u32[]{:S(2)}) copy-start(f32[2,4096]{1,0:T(2,128)} %param.11) | copy-start | bytes 98308
  11.4 13.1 %copy-start.2 = (f32[2,31,512]{2,0,1:T(2,128)S(1)}, f32[2,31,512]{2,0,1:T(2,128)}, u32[]{:S(2)}) copy-start(f32[2,31,512]{2,0,1:T(2,128)} %param.14) | copy-start | bytes 380932
  11.4 21.0 %copy-start.4 = (f32[2,512]{1,0:T(2,128)S(1)}, f32[2,512]{1,0:T(2,128)}, u32[]{:S(2)}) copy-start(f32[2,512]{1,0:T(2,128)} %param.15) | copy-start | bytes 12292
  11.5 243.6 %all-gather.17.cloned.1.call-start = ((), (), s32[]{:S(2)}) async-start(), calls=%async_computation.2 | async-start | bytes 5242880 | tf_op jit(solution)/shard_map/all_gather | solution.py:67
  14.6 321.1 %all-gather.21.cloned.1.call-start = ((), (), s32[]{:S(2)}) async-start(), calls=%async_computation.4 | async-start | bytes 5242880 | tf_op jit(solution)/shard_map/all_gather | solution.py:51
  15.2 401.2 %all-gather.19.cloned.1.call-start = ((), (), s32[]{:S(2)}) async-start(), calls=%async_computation.3 | async-start | bytes 5242880 | tf_op jit(solution)/shard_map/all_gather | solution.py:50
  15.8 481.3 %all-gather.23.cloned.1.call-start = ((), (), s32[]{:S(2)}) async-start(), calls=%async_computation.5 | async-start | bytes 5242880 | tf_op jit(solution)/shard_map/all_gather | solution.py:67
  15.9 8.7 %collective-permute-start = (bf16[224,1024]{1,0:T(8,128)(2,1)S(1)}, bf16[224,1024]{1,0:T(8,128)(2,1)S(1)}, u32[]{:S(2)}, u32[]{:S(2)}) collective-permute-start(bf16[224,1024]{1,0:T(8,128)(2,1)S(1)} %copy-done.1), channel_id=1, source_target_pairs={{0,1},{1,2},{2,3},{3,0},{4,5},{5,6},{6,7},{7,4},{8,9},{9,10},{10,1... | collective-permute-start | bytes 1376264 | tf_op jit(solution)/shard_map/ppermute | solution.py:43
  24.5 7.9 %collective-permute-start.1 = (bf16[224,1024]{1,0:T(8,128)(2,1)S(1)}, bf16[224,1024]{1,0:T(8,128)(2,1)S(1)}, u32[]{:S(2)}, u32[]{:S(2)}) collective-permute-start(bf16[224,1024]{1,0:T(8,128)(2,1)S(1)} %collective-permute-done), channel_id=1, source_target_pairs={{0,1},{1,2},{2,3},{3,0},{4,5},{5,6},{6,7},{7,4},{8,9},{9,10},{10,1... | collective-permute-start | bytes 1376264 | tf_op jit(solution)/shard_map/ppermute | solution.py:43
  32.4 8.0 %collective-permute-start.2 = (bf16[224,1024]{1,0:T(8,128)(2,1)S(1)}, bf16[224,1024]{1,0:T(8,128)(2,1)}, u32[]{:S(2)}, u32[]{:S(2)}) collective-permute-start(bf16[224,1024]{1,0:T(8,128)(2,1)S(1)} %collective-permute-done.1), channel_id=1, source_target_pairs={{0,1},{1,2},{2,3},{3,0},{4,5},{5,6},{6,7},{7,4},{8,9},{9,10},{10,1... | collective-permute-start | bytes 1376264 | tf_op jit(solution)/shard_map/ppermute | solution.py:43
  96.8 82.1 %copy-start.5 = (f32[2,512]{1,0:T(2,128)S(1)}, f32[2,512]{1,0:T(2,128)}, u32[]{:S(2)}) copy-start(f32[2,512]{1,0:T(2,128)} %param.16) | copy-start | bytes 12292
  177.6 2.9 collective-permute-start.3
  258.4 8.0 %collective-permute-start.4 = (bf16[224,1024]{1,0:T(8,128)(2,1)S(1)}, bf16[224,1024]{1,0:T(8,128)(2,1)S(1)}, u32[]{:S(2)}, u32[]{:S(2)}) collective-permute-start(bf16[224,1024]{1,0:T(8,128)(2,1)S(1)} %fusion.41), channel_id=1, source_target_pairs={{0,1},{1,2},{2,3},{3,0},{4,5},{5,6},{6,7},{7,4},{8,9},{9,10},{10,1... | collective-permute-start | bytes 1376264 | tf_op jit(solution)/shard_map/ppermute | solution.py:43
  266.3 7.9 %collective-permute-start.5 = (bf16[224,1024]{1,0:T(8,128)(2,1)S(1)}, bf16[224,1024]{1,0:T(8,128)(2,1)S(1)}, u32[]{:S(2)}, u32[]{:S(2)}) collective-permute-start(bf16[224,1024]{1,0:T(8,128)(2,1)S(1)} %collective-permute-done.4), channel_id=1, source_target_pairs={{0,1},{1,2},{2,3},{3,0},{4,5},{5,6},{6,7},{7,4},{8,9},{9,10},{10,1... | collective-permute-start | bytes 1376264 | tf_op jit(solution)/shard_map/ppermute | solution.py:43
  274.3 7.9 %collective-permute-start.6 = (bf16[224,1024]{1,0:T(8,128)(2,1)S(1)}, bf16[224,1024]{1,0:T(8,128)(2,1)S(1)}, u32[]{:S(2)}, u32[]{:S(2)}) collective-permute-start(bf16[224,1024]{1,0:T(8,128)(2,1)S(1)} %collective-permute-done.5), channel_id=1, source_target_pairs={{0,1},{1,2},{2,3},{3,0},{4,5},{5,6},{6,7},{7,4},{8,9},{9,10},{10,1... | collective-permute-start | bytes 1376264 | tf_op jit(solution)/shard_map/ppermute | solution.py:43
  419.9 2.9 collective-permute-start.7
Sparse Core Ops, SparseCore 0:
  9.9 83.4 all-gather.14
  95.0 79.2 all-gather.12
  175.8 79.2 all-gather.16
  256.5 79.2 all-gather.20
  337.2 79.2 all-gather.18
  417.9 79.2 all-gather.22
